TPU v7x, 32 devices: a whole 2x2x4 slice. The times are simulated.
32 devices in a mesh: sp: 8 (over z, x), tp: 4 (over y, core).
Axes of the slice: x: 2, y: 2, z: 4, core: 2. Of those that a mesh axis runs over, the one named last changes fastest.
Arguments:
- queries: bfloat16 [3072, 1024], P('sp', 'tp'), may hold values from -160 to 160
- key_vectors: bfloat16 [3072, 1024], P('sp', 'tp'), may hold values from -7 to 7
- values: bfloat16 [3072, 1024], P('sp', 'tp'), may hold values from -6 to 6
- head_lambda: float32 [8], P('tp'), may hold values from 0.3 to 0.8
- head_gain: float32 [128], replicated, may hold values from 0.1 to 1.9
- w_out: bfloat16 [1024, 2048], P('tp'), may hold values from -0.1875 to 0.1875
- residual: bfloat16 [3072, 2048], P(('sp', 'tp')), may hold values from -6 to 6
- ffn_gain: float32 [2048], replicated, may hold values from 0.1 to 1.9
- route_ids: int32 [3072, 2], P(('sp', 'tp')), may hold values from 0 to 7, all different within a row; in each aligned block of 96 rows (0 to 95, 96 to 191, ...) at most 30 rows name the same one
- route_logits: float32 [3072, 2], P(('sp', 'tp')), may hold values from -8 to 310
- w_gate: bfloat16 [8, 2048, 2048], P('sp', None, 'tp'), may hold values from -0.3125 to 0.3125
- w_up: bfloat16 [8, 2048, 2048], P('sp', None, 'tp'), may hold values from -0.3125 to 0.3125
- w_down: bfloat16 [8, 2048, 2048], P('sp', 'tp'), may hold values from -0.125 to 0.125
Outputs:
- layer_out: bfloat16 [3072, 2048], P(('sp', 'tp'))
Inputs may be any that keep to these rules, and one draw needn't show every extreme that they name: `route_ids`: in the rows of one device after the attention (aligned blocks of 96 rows) no expert is named by more than 30 rows, a bound that some block reaches while other experts in the same block get fewer rows; each row names 2 different experts.
All inputs are finite; a program needn't handle non-finite values.
Results may differ from a plain program's by a relative error of at most 0.023.
Values may be sent and summed in bfloat16 or wider, within the bound.
A program may use at most 192 MiB of HBM per device.

v0:
```python
import jax
import jax.numpy as jnp
from jax import lax
from jax.sharding import PartitionSpec as P

SEGMENT = 64
SEQUENCES = 1
EPS = 1e-06
NEG = -1e30
CLAMP = 7.0
ALPHA = 1.702
OUT_FACTOR = 0.8


def shards(
    queries,
    key_vectors,
    values,
    head_lambda,
    head_gain,
    w_out,
    residual,
    ffn_gain,
    route_ids,
    route_logits,
    w_gate,
    w_up,
    w_down,
):
    tok_count = queries.shape[0]
    local_heads = head_lambda.shape[0]
    head_width = queries.shape[1] // (2 * local_heads)
    value_width = values.shape[1] // local_heads
    score_scale = head_width ** (-0.5)
    n_tp = lax.axis_size("tp")
    n_sp = lax.axis_size("sp")
    seq_length = tok_count * n_sp // SEQUENCES
    query_pos = lax.axis_index("sp") * tok_count + jnp.arange(tok_count, dtype=jnp.int32)
    query_seg = query_pos // SEGMENT
    query_seq = query_pos // seq_length
    seq_begin = query_seq[0] * seq_length
    last_seg = query_seg[tok_count - 1]
    query_heads = queries.reshape(tok_count, local_heads, 2, head_width)

    def absorb(carry, key_block, value_block, key_start):
        maxima, totals, sums = carry
        block_len = key_block.shape[0]
        key_pos = key_start + jnp.arange(block_len, dtype=jnp.int32)
        visible = ((key_pos // SEGMENT)[None, :] <= query_seg[:, None]) & (
            (key_pos // seq_length)[None, :] == query_seq[:, None]
        )
        score = (
            jnp.einsum(
                "qhjd,khjd->jhqk", query_heads, key_block, preferred_element_type=jnp.float32
            )
            * score_scale
        )
        score = jnp.where(visible, score, NEG)
        new_max = jnp.maximum(maxima, jnp.max(score, axis=-1))
        expo = jnp.where(visible, jnp.exp(score - new_max[..., None]), 0.0)
        factor = jnp.exp(maxima - new_max)
        totals = totals * factor + jnp.sum(expo, axis=-1)
        added = jnp.einsum(
            "jhqk,khd->jqhd",
            expo.astype(jnp.bfloat16),
            value_block,
            preferred_element_type=jnp.float32,
        )
        sums = sums * jnp.transpose(factor, (0, 2, 1))[..., None] + added
        return (new_max, totals, sums)

    def maybe_absorb(carry, key_block, value_block, key_start):
        block_len = key_block.shape[0]
        needed = (key_start // SEGMENT <= last_seg) & (key_start + block_len - 1 >= seq_begin)
        return lax.cond(
            needed,
            lambda inner: absorb(inner, key_block, value_block, key_start),
            lambda inner: inner,
            carry,
        )

    initial = (
        jnp.full((2, local_heads, tok_count), NEG, jnp.float32),
        jnp.zeros((2, local_heads, tok_count), jnp.float32),
        jnp.zeros((2, tok_count, local_heads, value_width), jnp.float32),
    )
    key_piece = lax.all_gather(key_vectors, "sp", axis=0, tiled=True)
    value_piece = lax.all_gather(values, "sp", axis=0, tiled=True)
    piece_len = key_piece.shape[0]
    key_rows = key_piece.reshape(piece_len, local_heads, 2, head_width)
    value_rows = value_piece.reshape(piece_len, local_heads, value_width)
    key_step = 512

    def advance(block_index, inner):
        key_offset = block_index * key_step
        key_block = lax.dynamic_slice_in_dim(key_rows, key_offset, key_step, 0)
        value_block = lax.dynamic_slice_in_dim(value_rows, key_offset, key_step, 0)
        return maybe_absorb(inner, key_block, value_block, key_offset)

    maxima, totals, sums = lax.fori_loop(0, piece_len // key_step, advance, initial)
    attended = sums / jnp.transpose(totals, (0, 2, 1))[..., None]
    diff = attended[0] - head_lambda[None, :, None] * attended[1]
    scale_rows = lax.rsqrt(jnp.mean(diff * diff, axis=-1, keepdims=True) + EPS)
    head_rows = (diff * scale_rows * head_gain * OUT_FACTOR).astype(jnp.bfloat16)
    head_rows = head_rows.reshape(tok_count, local_heads * value_width)
    own_count = tok_count // n_tp
    whole_weight = lax.all_gather(w_out, "tp", axis=0, tiled=True)
    token_heads = lax.all_to_all(head_rows, "tp", split_axis=0, concat_axis=1, tiled=True)
    projected = jnp.dot(token_heads, whole_weight, preferred_element_type=jnp.float32)
    mixed = (residual.astype(jnp.float32) + projected).astype(jnp.bfloat16)
    mixed32 = mixed.astype(jnp.float32)
    normed = (
        mixed32 * lax.rsqrt(jnp.mean(mixed32 * mixed32, axis=-1, keepdims=True) + EPS) * ffn_gain
    ).astype(jnp.bfloat16)
    gates = jax.nn.softmax(route_logits, axis=-1)
    top_count = route_ids.shape[1]
    model_width = normed.shape[1]
    cap_slots = max(2, 5 * top_count * tok_count // (4 * n_tp * n_sp))
    flat_ids = route_ids.reshape(-1)
    chosen = (flat_ids[:, None] == jnp.arange(n_sp, dtype=jnp.int32)[None, :]).astype(jnp.int32)
    earlier = jnp.cumsum(chosen, axis=0) - chosen
    slot_rank = jnp.sum(earlier * chosen, axis=1)
    slot_index = flat_ids * cap_slots + slot_rank
    source_rows = jnp.repeat(normed, top_count, axis=0)
    outgoing = (
        jnp.zeros((n_sp * cap_slots, model_width), jnp.bfloat16).at[slot_index].set(source_rows)
    )
    outgoing = outgoing.reshape(n_sp, cap_slots, model_width)
    arrived = lax.all_to_all(outgoing, "sp", split_axis=0, concat_axis=0, tiled=True)
    senders, slot_count, arrived_width = arrived.shape
    flat_in = arrived.reshape(senders * slot_count, arrived_width)
    piece = lax.all_gather(flat_in, "tp", axis=0, tiled=True)
    gate_pre = jnp.dot(piece, w_gate[0], preferred_element_type=jnp.float32)
    up_pre = jnp.dot(piece, w_up[0], preferred_element_type=jnp.float32)
    gate_cut = jnp.minimum(gate_pre, CLAMP)
    up_cut = jnp.clip(up_pre, -CLAMP, CLAMP)
    active = (gate_cut * jax.nn.sigmoid(ALPHA * gate_cut) * (up_cut + 1.0)).astype(jnp.bfloat16)
    reduced = lax.psum_scatter(
        jnp.dot(active, w_down[0], preferred_element_type=jnp.float32).astype(jnp.bfloat16),
        "tp",
        scatter_dimension=0,
        tiled=True,
    )
    reduced = reduced.reshape(senders, slot_count, arrived_width)
    returned = lax.all_to_all(reduced, "sp", split_axis=0, concat_axis=0, tiled=True)
    picked = returned.reshape(n_sp * cap_slots, model_width)[slot_index].astype(jnp.float32)
    weighted = (picked * gates.reshape(-1)[:, None]).reshape(own_count, top_count, model_width)
    return (mixed32 + jnp.sum(weighted, axis=1)).astype(jnp.bfloat16)


def solution(mesh):
    in_specs = (
        P("sp", "tp"),
        P("sp", "tp"),
        P("sp", "tp"),
        P("tp"),
        P(),
        P("tp", None),
        P(("sp", "tp"), None),
        P(),
        P(("sp", "tp"), None),
        P(("sp", "tp"), None),
        P("sp", None, "tp"),
        P("sp", None, "tp"),
        P("sp", "tp", None),
    )
    out_specs = P(("sp", "tp"), None)
    return jax.shard_map(shards, mesh=mesh, in_specs=in_specs, out_specs=out_specs, check_vma=False)
```

profile of v0, /device:TPU:0, one launch (start us, length us, event | category | flops | bytes accessed | tf_op | source)
XLA Modules:
  0.0 338.7 jit_solution(3574506045380296739)
XLA Ops:
  6.6 1.9 copy.37
  8.6 1.8 copy.39
  10.4 0.7 all-gather.9.cloned.1.call-update
  11.1 0.5 slice.22
  11.6 0.6 slice.21
  12.7 0.6 reduce-window.6
  14.6 42.0 %all-gather.5.cloned.1.call-done = bf16[3072,256]{0,1:T(8,128)(2,1)} async-done(((bf16[384,256]{0,1:T(8,128)(2,1)}), bf16[3072,256]{0,1:T(8,128)(2,1)}) %all-gather.5.cloned.1.call-update) | async-done | bytes 1572880 | tf_op jit(solution)/shard_map/all_gather | solution.py:87
  56.6 2.7 copy.40
  59.3 42.0 %all-gather.7.cloned.1.call-done = bf16[3072,256]{0,1:T(8,128)(2,1)} async-done(((bf16[384,256]{0,1:T(8,128)(2,1)}), bf16[3072,256]{0,1:T(8,128)(2,1)}) %all-gather.7.cloned.1.call-update) | async-done | bytes 1572880 | tf_op jit(solution)/shard_map/all_gather | solution.py:88
  101.3 2.6 copy.42
  104.0 9.5 %while.24 = (s32[]{:T(128)}, f32[2,2,384]{2,1,0:T(2,128)S(1)}, f32[2,2,384]{2,1,0:T(2,128)S(1)}, f32[2,384,2,128]{3,1,0,2:T(8,128)S(1)}, s32[]{:T(128)}, /*index...) while((s32[]{:T(128)}, f32[2,2,384]{2,1,0:T(2,128)S(1)}, ...), condition=%wide.region_5.6_spmd.clone.clone, body=%wide.region_0.5_spmd.clone.clone.sunk | while | flops 310077472 | bytes 12468234 | solution.py:100
  104.7 4.9 %conditional.4 = ((f32[2,2,384]{2,1,0:T(2,128)S(1)}, f32[2,2,384]{2,1,0:T(2,128)S(1)}, f32[2,384,2,128]{3,1,0,2:T(8,128)S(1)})) conditional(s32[]{:T(128)} %convert_element_type.87, (f32[2,2,384]{2,1,0:T(2,128)S(1)}, f32[2,2,384]{2,1,0:T(2,128)S(1)}, f32[2,384,2,128]{3,1,0,2:T(8,128)S(1)}) %tuple.101, (s32[]{:T(128)}, ...), branch_computations={%region_1.1_spmd, %region_2.4_spmd.clone} | conditional | flops 310070912 | bytes 12456133 | solution.py:75
  105.1 1.7 fusion.4
  106.8 0.9 fusion.5
  107.7 1.9 fusion.12
  113.4 0.3 broadcast_divide_fusion
  113.7 0.9 copy-done.1
  114.6 0.8 fusion.59
  115.4 0.3 copy.45
  115.7 1.1 squeeze.24
  116.8 1.3 copy.46
  118.1 1.1 squeeze.25
  119.6 0.5 mul.176
  120.1 0.3 mul.177
  120.4 1.8 multiply_convert_fusion.2
  122.2 3.4 all-to-all-start
  125.6 7.7 %all-to-all-done = bf16[4,96,256]{2,1,0:T(8,128)(2,1)S(1)} async-done(((bf16[4,96,256]{2,1,0:T(8,128)(2,1)}), bf16[4,96,256]{2,1,0:T(8,128)(2,1)S(1)}, u32[]{:S(2)}, u32[]{:S(2)}) %all-to-all-start) | async-done | bytes 196640 | tf_op jit(solution)/shard_map/all_to_all | solution.py:108
  133.3 4.3 %all-gather.9.cloned.1.call-done = bf16[1024,2048]{1,0:T(8,128)(2,1)} async-done(((bf16[256,2048]{1,0:T(8,128)(2,1)}), bf16[1024,2048]{1,0:T(8,128)(2,1)}) %all-gather.9.cloned.1.call-update) | async-done | bytes 4194320 | tf_op jit(solution)/shard_map/all_gather | solution.py:107
  137.6 3.2 multiply_reduce_fusion.1
  140.9 0.9 copy-done.3
  141.9 0.5 broadcast_in_dim.57
  142.4 1.2 reshape.176
  143.6 3.3 scatter_custom_fusion
  146.9 1.5 reshape.158
  148.4 45.5 %all_to_all.26 = bf16[8,30,2048]{2,1,0:T(8,128)(2,1)} all-to-all(bf16[8,30,2048]{2,1,0:T(8,128)(2,1)S(1)} %reshape.158), channel_id=1, replica_groups=mesh['sp'=8,'tp'=4] {'sp'}, dimensions={0} | all-to-all | bytes 1966080 | tf_op jit(solution)/shard_map/all_to_all | solution.py:129
  193.9 2.4 reshape.159
  196.6 31.4 %all-gather.11.cloned.1.call-done = bf16[960,2048]{1,0:T(8,128)(2,1)} async-done(((bf16[240,2048]{1,0:T(8,128)(2,1)}), bf16[960,2048]{1,0:T(8,128)(2,1)}) %all-gather.11.cloned.1.call-update) | async-done | bytes 3932176 | tf_op jit(solution)/shard_map/all_gather | solution.py:132
  228.0 6.3 %fusion.35 = f32[960,512]{1,0:T(8,128)} fusion(bf16[960,2048]{1,0:T(8,128)(2,1)} %all-gather.11.cloned.1.call-done, bf16[1,2048,512]{2,1,0:T(8,128)(2,1)} %param.28), kind=kOutput, calls=%fused_computation.54 | convolution fusion | flops 2013265920 | bytes 7995392 | tf_op jit(solution)/shard_map/dot_general | solution.py:134
  234.4 9.8 %convolution_convert_fusion = bf16[960,2048]{1,0:T(8,128)(2,1)} fusion(bf16[1,512,2048]{2,1,0:T(8,128)(2,1)S(1)} %copy-done, f32[960,512]{1,0:T(8,128)} %fusion.35, bf16[960,2048]{1,0:T(8,128)(2,1)} %all-gather.11.cloned.1.call-done, bf16[1,2048,512]{2,1,0:T(8,128)(2,1)} %param.27), kind=kOutput, calls=%fused_computation.49 | convolution fusion | flops 4033413120 | bytes 14024704 | tf_op jit(solution)/shard_map/dot_general | solution.py:139
  244.3 43.0 %reduce-scatter.2.cloned.1.call-done = bf16[240,2048]{1,0:T(8,128)(2,1)} async-done(((bf16[960,2048]{1,0:T(8,128)(2,1)}), bf16[240,2048]{1,0:T(8,128)(2,1)}) %reduce-scatter.2.cloned.1.call-update) | async-done | bytes 983056 | tf_op jit(solution)/shard_map/reduce_scatter | solution.py:138
  287.3 2.4 reshape.160
  289.7 5.5 %all-to-all-start.2 = ((bf16[8,30,2048]{2,1,0:T(8,128)(2,1)}), bf16[8,30,2048]{2,1,0:T(8,128)(2,1)}, u32[]{:S(2)}, u32[]{:S(2)}) async-start(bf16[8,30,2048]{2,1,0:T(8,128)(2,1)} %reshape.160), calls=%async_computation.3 | async-start | bytes 2097152 | tf_op jit(solution)/shard_map/all_to_all | solution.py:145
  295.4 25.6 %all-to-all-done.2 = bf16[8,30,2048]{2,1,0:T(8,128)(2,1)} async-done(((bf16[8,30,2048]{2,1,0:T(8,128)(2,1)}), bf16[8,30,2048]{2,1,0:T(8,128)(2,1)}, u32[]{:S(2)}, u32[]{:S(2)}) %all-to-all-start.2) | async-done | bytes 983072 | tf_op jit(solution)/shard_map/all_to_all | solution.py:145
  321.0 1.5 reshape.161
  322.5 2.0 gather_fusion
  324.5 3.0 reshape.163
  327.6 3.7 %multiply_reduce_fusion = f32[96,2048]{1,0:T(8,128)S(1)} fusion(f32[96,2,2048]{2,1,0:T(2,128)} %reshape.163, f32[96,2]{1,0:T(8,128)S(1)} %copy.51), kind=kLoop, calls=%fused_computation.59 | loop fusion | flops 589824 | bytes 2360064 | tf_op jit(solution)/shard_map/reduce_sum | solution.py:148
  331.3 0.8 add_convert_fusion
  (111 shorter events, 3.1 us)
Async XLA Ops:
  6.5 227.8 %copy-start = (bf16[1,512,2048]{2,1,0:T(8,128)(2,1)S(1)}, bf16[1,512,2048]{2,1,0:T(8,128)(2,1)}, u32[]{:S(2)}) copy-start(bf16[1,512,2048]{2,1,0:T(8,128)(2,1)} %param.29) | copy-start | bytes 6291460
  6.5 5.7 %copy-start.6 = (bf16[384,256]{1,0:T(8,128)(2,1)S(1)}, bf16[384,256]{1,0:T(8,128)(2,1)}, u32[]{:S(2)}) copy-start(bf16[384,256]{1,0:T(8,128)(2,1)} %param.17) | copy-start | bytes 589828
  6.5 5.9 %copy-start.9 = (s32[96,2]{0,1:T(2,128)S(1)}, s32[96,2]{0,1:T(2,128)}, u32[]{:S(2)}) copy-start(s32[96,2]{0,1:T(2,128)} %param.25) | copy-start | bytes 2308
  6.5 8.0 %copy-start.10 = (f32[2]{0:T(128)S(1)}, f32[2]{0:T(128)}, u32[]{:S(2)}) copy-start(f32[2]{0:T(128)} %param.20) | copy-start | bytes 28
  6.5 8.0 %copy-start.11 = (f32[128]{0:T(128)S(1)}, f32[128]{0:T(128)}, u32[]{:S(2)}) copy-start(f32[128]{0:T(128)} %param.21) | copy-start | bytes 1540
  6.5 50.0 %all-gather.5.cloned.1.call-start = ((), (), s32[]{:S(2)}) async-start(), calls=%async_computation.4 | async-start | bytes 1769472 | tf_op jit(solution)/shard_map/all_gather | solution.py:87
  8.5 92.8 %all-gather.7.cloned.1.call-start = ((), (), s32[]{:S(2)}) async-start(), calls=%async_computation.5 | async-start | bytes 1769472 | tf_op jit(solution)/shard_map/all_gather | solution.py:88
  10.3 127.3 %all-gather.9.cloned.1.call-start = ((), (), s32[]{:S(2)}) async-start(), calls=%async_computation.6 | async-start | bytes 5242880 | tf_op jit(solution)/shard_map/all_gather | solution.py:107
  113.7 0.9 copy-start.1
  115.4 3.8 %copy-start.2 = (f32[2,384,2,128]{3,1,0,2:T(8,128)S(1)}, f32[2,384,2,128]{3,1,0,2:T(8,128)}, u32[]{:S(2)}) copy-start(f32[2,384,2,128]{3,1,0,2:T(8,128)} %copy-done.1) | copy-start | bytes 2359300
  119.2 1.2 copy-start.5
  122.2 11.2 %all-to-all-start = ((bf16[4,96,256]{2,1,0:T(8,128)(2,1)}), bf16[4,96,256]{2,1,0:T(8,128)(2,1)S(1)}, u32[]{:S(2)}, u32[]{:S(2)}) async-start(bf16[4,96,256]{2,1,0:T(8,128)(2,1)} %multiply_convert_fusion.2), calls=%async_computation | async-start | bytes 393216 | tf_op jit(solution)/shard_map/all_to_all | solution.py:108
  125.5 102.5 %all-gather.11.cloned.1.call-start = ((), (), s32[]{:S(2)}) async-start(), calls=%async_computation.7 | async-start | bytes 4915200 | tf_op jit(solution)/shard_map/all_gather | solution.py:132
  137.6 4.1 %copy-start.8 = (f32[2048]{0:T(1024)S(1)}, f32[2048]{0:T(1024)}, u32[]{:S(2)}) copy-start(f32[2048]{0:T(1024)} %param.24) | copy-start | bytes 24580
  140.8 0.9 copy-start.3
  196.4 90.9 %reduce-scatter.2.cloned.1.call-start = ((), (), s32[]{:S(2)}) async-start(), calls=%async_computation.8 | async-start | bytes 4915200 | tf_op jit(solution)/shard_map/reduce_scatter | solution.py:138
  244.2 51.0 %copy-start.7 = (f32[96,2]{0,1:T(2,128)S(1)}, f32[96,2]{0,1:T(2,128)}, u32[]{:S(2)}) copy-start(f32[96,2]{0,1:T(2,128)} %param.26) | copy-start | bytes 2308
  289.7 31.3 %all-to-all-start.2 = ((bf16[8,30,2048]{2,1,0:T(8,128)(2,1)}), bf16[8,30,2048]{2,1,0:T(8,128)(2,1)}, u32[]{:S(2)}, u32[]{:S(2)}) async-start(bf16[8,30,2048]{2,1,0:T(8,128)(2,1)} %reshape.160), calls=%async_computation.3 | async-start | bytes 2097152 | tf_op jit(solution)/shard_map/all_to_all | solution.py:145
  324.5 6.8 %copy-start.4 = (f32[96,2048]{1,0:T(8,128)S(1)}, f32[96,2048]{1,0:T(8,128)}, u32[]{:S(2)}) copy-start(f32[96,2048]{1,0:T(8,128)} %copy-done.3) | copy-start | bytes 2359300
Sparse Core Ops, SparseCore 0:
  9.4 47.1 all-gather.4
  58.6 42.5 all-gather.6
  102.9 34.7 all-gather.8
  196.5 31.4 all-gather.10
  244.4 42.8 reduce-scatter.1
where the time goes:
time: 340 us; the launch traced here: 339 us
  waiting for transfers between devices  197 us (58%)
  blocking collectives  45.5 us (13%)
  local copies, waits for them, and re-layouts  36.4 us (11%)
  matrix products  22.9 us (7%)
  between operations  14.1 us (4%)
  starting transfers between devices  9.27 us (3%)
  other arithmetic  9.27 us (3%)
  loops' own time  4.41 us (1%)
    all_to_all x1, blocking collectives, shards(): lax.all_to_all(outgoing, 'sp', split_axis=0, concat_axis=0, tiled=True)  45.5 us
    reduce_scatter x1, waiting for transfers between devices, shards(): lax.psum_scatter(jnp.dot(active, w_down[0], preferred_element_type=jnp.fl...  43 us
    all_gather x1, waiting for transfers between devices, shards(): value_piece = lax.all_gather(values, 'sp', axis=0, tiled=True)  42 us
    all_gather x1, waiting for transfers between devices, shards(): key_piece = lax.all_gather(key_vectors, 'sp', axis=0, tiled=True)  42 us
    all_gather x1, waiting for transfers between devices, shards(): piece = lax.all_gather(flat_in, 'tp', axis=0, tiled=True)  31.4 us
    all_to_all x1, waiting for transfers between devices, shards(): lax.all_to_all(reduced, 'sp', split_axis=0, concat_axis=0, tiled=True)  25.6 us
    unnamed x31, local copies, waits for them, and re-layouts  11 us
    dot_general x1, matrix products, shards(): jnp.dot(active, w_down[0], preferred_element_type=jnp.float32)  9.84 us
  transfers between devices with their start and end apart: 7, of which 7 were waited for; matrix products, arithmetic and copies ran while one was open for 7% of the time, Pallas kernels for 0%

commit v1 on v0

--- a/solution.py
+++ b/solution.py
@@ -85,7 +85,21 @@
         jnp.zeros((2, tok_count, local_heads, value_width), jnp.float32),
     )
     key_piece = lax.all_gather(key_vectors, "sp", axis=0, tiled=True)
-    value_piece = lax.all_gather(values, "sp", axis=0, tiled=True)
+
+    def perform_column(arr):
+        group_axis = "sp"
+        cores_n = lax.axis_size(group_axis)
+        y_new = sorted(((s, (s + 1) % cores_n) for s in range(cores_n)))
+        extra = arr
+        in_order = [extra]
+        for ii in range(1, cores_n):
+            extra = lax.ppermute(extra, group_axis, y_new)
+            in_order.insert(0, extra)
+        z1 = jnp.concatenate(in_order, 0)
+        response = jnp.roll(z1, (lax.axis_index(group_axis) + 1) * arr.shape[0], 0)
+        return response
+
+    value_piece = perform_column(values)
     piece_len = key_piece.shape[0]
     key_rows = key_piece.reshape(piece_len, local_heads, 2, head_width)
     value_rows = value_piece.reshape(piece_len, local_heads, value_width)

time: 340 us -> 330 us (0.971)
  waiting for transfers between devices: 197 us -> 171 us
  local copies, waits for them, and re-layouts: 36.4 us -> 43.2 us
  blocking collectives: 45.5 us -> 50.6 us
    ppermute x0 -> x7, waiting for transfers between devices: none -> 65.3 us  [perform_column(): extra = lax.ppermute(extra, group_axis, y_new)]
    all_gather x1 -> x0, waiting for transfers between devices: 42 us -> none  [shards(): value_piece = lax.all_gather(values, 'sp', axis=0, tiled=True)]
    all_gather x1, waiting for transfers between devices: 42 us -> 0.01 us  [shards(): key_piece = lax.all_gather(key_vectors, 'sp', axis=0, tiled=True)]
    all_to_all x1, blocking collectives: 45.5 us -> 50.6 us  [shards(): lax.all_to_all(outgoing, 'sp', split_axis=0, concat_axis=0, tiled=True)]
    unnamed x31 -> x42, local copies, waits for them, and re-layouts: 11 us -> 15.9 us
    all_gather x1, waiting for transfers between devices: 4.3 us -> 0.02 us  [shards(): whole_weight = lax.all_gather(w_out, 'tp', axis=0, tiled=True)]
  transfers between devices with their start and end apart: 7 -> 13, of which waited for: 7 -> 11; matrix products, arithmetic and copies ran while one was open for 7% -> 9% of each run, Pallas kernels for 0% -> 0%
where the time goes in v1:
time: 330 us; the launch traced here: 328 us
  waiting for transfers between devices  171 us (52%)
  blocking collectives  50.6 us (15%)
  local copies, waits for them, and re-layouts  43.2 us (13%)
  matrix products  22.8 us (7%)
  between operations  14.1 us (4%)
  starting transfers between devices  12.4 us (4%)
  other arithmetic  10.1 us (3%)
  loops' own time  4.4 us (1%)
    ppermute x7, waiting for transfers between devices, perform_column(): extra = lax.ppermute(extra, group_axis, y_new)  65.3 us
    all_to_all x1, blocking collectives, shards(): lax.all_to_all(outgoing, 'sp', split_axis=0, concat_axis=0, tiled=True)  50.6 us
    reduce_scatter x1, waiting for transfers between devices, shards(): lax.psum_scatter(jnp.dot(active, w_down[0], preferred_element_type=jnp.fl...  43.1 us
    all_gather x1, waiting for transfers between devices, shards(): piece = lax.all_gather(flat_in, 'tp', axis=0, tiled=True)  31.6 us
    all_to_all x1, waiting for transfers between devices, shards(): lax.all_to_all(reduced, 'sp', split_axis=0, concat_axis=0, tiled=True)  25.6 us
    unnamed x42, local copies, waits for them, and re-layouts  15.9 us
    dot_general x1, matrix products, shards(): jnp.dot(active, w_down[0], preferred_element_type=jnp.float32)  9.83 us
  transfers between devices with their start and end apart: 13, of which 11 were waited for; matrix products, arithmetic and copies ran while one was open for 9% of the time, Pallas kernels for 0%

profile of v1, /device:TPU:0, one launch (start us, length us, event | category | flops | bytes accessed | tf_op | source)
XLA Modules:
  0.0 328.2 jit_solution(12206187334356444840)
XLA Ops:
  6.5 1.9 copy.39
  8.5 1.1 copy.41
  9.6 3.0 collective-permute-start
  13.6 7.0 %collective-permute-done = bf16[384,256]{0,1:T(8,128)(2,1)S(1)} collective-permute-done((bf16[384,256]{0,1:T(8,128)(2,1)S(1)}, bf16[384,256]{0,1:T(8,128)(2,1)S(1)}, u32[]{:S(2)}, u32[]{:S(2)}) %collective-permute-start) | collective-permute-done | bytes 196640 | tf_op jit(solution)/shard_map/ppermute | solution.py:96
  20.6 12.6 %collective-permute-done.1 = bf16[384,256]{0,1:T(8,128)(2,1)S(1)} collective-permute-done((bf16[384,256]{0,1:T(8,128)(2,1)S(1)}, bf16[384,256]{0,1:T(8,128)(2,1)S(1)}, u32[]{:S(2)}, u32[]{:S(2)}) %collective-permute-start.1) | collective-permute-done | bytes 196640 | tf_op jit(solution)/shard_map/ppermute | solution.py:96
  34.0 7.5 %collective-permute-done.2 = bf16[384,256]{0,1:T(8,128)(2,1)S(1)} collective-permute-done((bf16[384,256]{0,1:T(8,128)(2,1)S(1)}, bf16[384,256]{0,1:T(8,128)(2,1)S(1)}, u32[]{:S(2)}, u32[]{:S(2)}) %collective-permute-start.2) | collective-permute-done | bytes 196640 | tf_op jit(solution)/shard_map/ppermute | solution.py:96
  41.6 13.4 %collective-permute-done.3 = bf16[384,256]{0,1:T(8,128)(2,1)S(1)} collective-permute-done((bf16[384,256]{0,1:T(8,128)(2,1)S(1)}, bf16[384,256]{0,1:T(8,128)(2,1)S(1)}, u32[]{:S(2)}, u32[]{:S(2)}) %collective-permute-start.3) | collective-permute-done | bytes 196640 | tf_op jit(solution)/shard_map/ppermute | solution.py:96
  55.7 10.8 %collective-permute-done.4 = bf16[384,256]{0,1:T(8,128)(2,1)S(1)} collective-permute-done((bf16[384,256]{0,1:T(8,128)(2,1)S(1)}, bf16[384,256]{0,1:T(8,128)(2,1)S(1)}, u32[]{:S(2)}, u32[]{:S(2)}) %collective-permute-start.4) | collective-permute-done | bytes 196640 | tf_op jit(solution)/shard_map/ppermute | solution.py:96
  67.7 1.7 copy.40
  69.5 0.9 copy.45
  71.3 5.5 %collective-permute-done.5 = bf16[384,256]{0,1:T(8,128)(2,1)} collective-permute-done((bf16[384,256]{0,1:T(8,128)(2,1)S(1)}, bf16[384,256]{0,1:T(8,128)(2,1)}, u32[]{:S(2)}, u32[]{:S(2)}) %collective-permute-start.5) | collective-permute-done | bytes 196640 | tf_op jit(solution)/shard_map/ppermute | solution.py:96
  76.8 8.5 %collective-permute-done.6 = bf16[384,256]{0,1:T(8,128)(2,1)S(1)} collective-permute-done((bf16[384,256]{0,1:T(8,128)(2,1)}, bf16[384,256]{0,1:T(8,128)(2,1)S(1)}, u32[]{:S(2)}, u32[]{:S(2)}) %collective-permute-start.6) | collective-permute-done | bytes 196640 | tf_op jit(solution)/shard_map/ppermute | solution.py:96
  85.4 1.0 constant_dynamic-update-slice_fusion.14
  86.7 1.0 constant_dynamic-update-slice_fusion.6
  87.9 1.8 constant_dynamic-slice_fusion
  89.7 2.6 copy.46
  92.3 2.7 copy.44
  95.1 9.4 %while.24 = (s32[]{:T(128)}, f32[2,2,384]{2,1,0:T(2,128)S(1)}, f32[2,2,384]{2,1,0:T(2,128)S(1)}, f32[2,384,2,128]{3,1,0,2:T(8,128)S(1)}, s32[]{:T(128)}, /*index...) while((s32[]{:T(128)}, f32[2,2,384]{2,1,0:T(2,128)S(1)}, ...), condition=%wide.region_5.6_spmd.clone.clone, body=%wide.region_0.5_spmd.clone.clone.sunk | while | flops 310077472 | bytes 12468234 | solution.py:114
  95.8 4.9 %conditional.4 = ((f32[2,2,384]{2,1,0:T(2,128)S(1)}, f32[2,2,384]{2,1,0:T(2,128)S(1)}, f32[2,384,2,128]{3,1,0,2:T(8,128)S(1)})) conditional(s32[]{:T(128)} %convert_element_type.87, (f32[2,2,384]{2,1,0:T(2,128)S(1)}, f32[2,2,384]{2,1,0:T(2,128)S(1)}, f32[2,384,2,128]{3,1,0,2:T(8,128)S(1)}) %tuple.101, (s32[]{:T(128)}, ...), branch_computations={%region_1.1_spmd, %region_2.4_spmd.clone} | conditional | flops 310070912 | bytes 12456133 | solution.py:75
  96.2 1.7 fusion.4
  97.9 0.9 fusion.5
  98.8 1.9 fusion.12
  104.8 0.9 copy-done.1
  106.8 1.1 squeeze.24
  107.9 1.3 copy.50
  109.2 1.1 squeeze.25
  111.5 1.9 multiply_convert_fusion.2
  113.4 3.5 %all-to-all-start = ((bf16[4,96,256]{2,1,0:T(8,128)(2,1)}), bf16[4,96,256]{2,1,0:T(8,128)(2,1)S(1)}, u32[]{:S(2)}, u32[]{:S(2)}) async-start(bf16[4,96,256]{2,1,0:T(8,128)(2,1)} %multiply_convert_fusion.2), calls=%async_computation | async-start | bytes 393216 | tf_op jit(solution)/shard_map/all_to_all | solution.py:122
  117.1 5.0 %all-to-all-done = bf16[4,96,256]{2,1,0:T(8,128)(2,1)S(1)} async-done(((bf16[4,96,256]{2,1,0:T(8,128)(2,1)}), bf16[4,96,256]{2,1,0:T(8,128)(2,1)S(1)}, u32[]{:S(2)}, u32[]{:S(2)}) %all-to-all-start) | async-done | bytes 196640 | tf_op jit(solution)/shard_map/all_to_all | solution.py:122
  122.2 3.1 multiply_reduce_fusion.1
  125.3 0.9 copy-done.3
  126.8 1.2 reshape.176
  128.0 3.3 %scatter_custom_fusion = bf16[240,2048]{1,0:T(8,128)(2,1)} fusion(s32[192]{0:T(256)S(1)} %bitcast.84, bf16[192,2048]{1,0:T(8,128)(2,1)} %reshape.176, bf16[]{:T(256)} %constant.252.clone.1), kind=kCustom, calls=%fused_computation.63 | custom fusion | bytes 983552 | tf_op jit(solution)/shard_map/scatter | solution.py:140
  131.4 1.5 reshape.158
  132.9 50.6 %all_to_all.26 = bf16[8,30,2048]{2,1,0:T(8,128)(2,1)} all-to-all(bf16[8,30,2048]{2,1,0:T(8,128)(2,1)S(1)} %reshape.158), channel_id=1, replica_groups=mesh['sp'=8,'tp'=4] {'sp'}, dimensions={0} | all-to-all | bytes 1966080 | tf_op jit(solution)/shard_map/all_to_all | solution.py:143
  183.4 2.4 reshape.159
  186.0 31.6 %all-gather.8.cloned.1.call-done = bf16[960,2048]{1,0:T(8,128)(2,1)} async-done(((bf16[240,2048]{1,0:T(8,128)(2,1)}), bf16[960,2048]{1,0:T(8,128)(2,1)}) %all-gather.8.cloned.1.call-update) | async-done | bytes 3932176 | tf_op jit(solution)/shard_map/all_gather | solution.py:146
  217.5 6.3 %fusion.35 = f32[960,512]{1,0:T(8,128)} fusion(bf16[960,2048]{1,0:T(8,128)(2,1)} %all-gather.8.cloned.1.call-done, bf16[1,2048,512]{2,1,0:T(8,128)(2,1)} %param.28), kind=kOutput, calls=%fused_computation.54 | convolution fusion | flops 2013265920 | bytes 7995392 | tf_op jit(solution)/shard_map/dot_general | solution.py:148
  223.9 9.8 %convolution_convert_fusion = bf16[960,2048]{1,0:T(8,128)(2,1)} fusion(bf16[1,512,2048]{2,1,0:T(8,128)(2,1)S(1)} %copy-done, f32[960,512]{1,0:T(8,128)} %fusion.35, bf16[960,2048]{1,0:T(8,128)(2,1)} %all-gather.8.cloned.1.call-done, bf16[1,2048,512]{2,1,0:T(8,128)(2,1)} %param.27), kind=kOutput, calls=%fused_computation.49 | convolution fusion | flops 4033413120 | bytes 14024704 | tf_op jit(solution)/shard_map/dot_general | solution.py:153
  233.7 43.1 %reduce-scatter.2.cloned.1.call-done = bf16[240,2048]{1,0:T(8,128)(2,1)} async-done(((bf16[960,2048]{1,0:T(8,128)(2,1)}), bf16[240,2048]{1,0:T(8,128)(2,1)}) %reduce-scatter.2.cloned.1.call-update) | async-done | bytes 983056 | tf_op jit(solution)/shard_map/reduce_scatter | solution.py:152
  276.8 2.4 reshape.160
  279.3 5.5 %all-to-all-start.2 = ((bf16[8,30,2048]{2,1,0:T(8,128)(2,1)}), bf16[8,30,2048]{2,1,0:T(8,128)(2,1)}, u32[]{:S(2)}, u32[]{:S(2)}) async-start(bf16[8,30,2048]{2,1,0:T(8,128)(2,1)} %reshape.160), calls=%async_computation.3 | async-start | bytes 2097152 | tf_op jit(solution)/shard_map/all_to_all | solution.py:159
  285.0 25.6 %all-to-all-done.2 = bf16[8,30,2048]{2,1,0:T(8,128)(2,1)} async-done(((bf16[8,30,2048]{2,1,0:T(8,128)(2,1)}), bf16[8,30,2048]{2,1,0:T(8,128)(2,1)}, u32[]{:S(2)}, u32[]{:S(2)}) %all-to-all-start.2) | async-done | bytes 983072 | tf_op jit(solution)/shard_map/all_to_all | solution.py:159
  310.6 1.5 reshape.161
  312.0 2.0 gather_fusion
  314.1 3.0 reshape.163
  317.1 3.7 %multiply_reduce_fusion = f32[96,2048]{1,0:T(8,128)S(1)} fusion(f32[96,2,2048]{2,1,0:T(2,128)} %reshape.163, f32[96,2]{1,0:T(8,128)S(1)} %copy.55), kind=kLoop, calls=%fused_computation.59 | loop fusion | flops 589824 | bytes 2360064 | tf_op jit(solution)/shard_map/reduce_sum | solution.py:162
  320.9 0.8 add_convert_fusion
  (135 shorter events, 9.1 us)
Async XLA Ops:
  6.5 217.4 %copy-start = (bf16[1,512,2048]{2,1,0:T(8,128)(2,1)S(1)}, bf16[1,512,2048]{2,1,0:T(8,128)(2,1)}, u32[]{:S(2)}) copy-start(bf16[1,512,2048]{2,1,0:T(8,128)(2,1)} %param.29) | copy-start | bytes 6291460
  6.5 70.2 %copy-start.8 = (f32[2]{0:T(128)S(1)}, f32[2]{0:T(128)}, u32[]{:S(2)}) copy-start(f32[2]{0:T(128)} %param.20) | copy-start | bytes 28
  6.5 70.2 %copy-start.9 = (f32[128]{0:T(128)S(1)}, f32[128]{0:T(128)}, u32[]{:S(2)}) copy-start(f32[128]{0:T(128)} %param.21) | copy-start | bytes 1540
  6.5 85.8 %all-gather.4.cloned.1.call-start = ((), (), s32[]{:S(2)}) async-start(), calls=%async_computation.4 | async-start | bytes 1769472 | tf_op jit(solution)/shard_map/all_gather | solution.py:87
  8.5 113.7 %all-gather.6.cloned.1.call-start = ((), (), s32[]{:S(2)}) async-start(), calls=%async_computation.5 | async-start | bytes 5242880 | tf_op jit(solution)/shard_map/all_gather | solution.py:121
  9.6 11.0 %collective-permute-start = (bf16[384,256]{0,1:T(8,128)(2,1)S(1)}, bf16[384,256]{0,1:T(8,128)(2,1)S(1)}, u32[]{:S(2)}, u32[]{:S(2)}) collective-permute-start(bf16[384,256]{0,1:T(8,128)(2,1)S(1)} %copy.41), channel_id=1, source_target_pairs={{0,4},{4,8},{8,12},{12,16},{16,20},{20,24},{24,28},{28,0},{1,5},{5... | collective-permute-start | bytes 589832 | tf_op jit(solution)/shard_map/ppermute | solution.py:96
  20.6 12.6 %collective-permute-start.1 = (bf16[384,256]{0,1:T(8,128)(2,1)S(1)}, bf16[384,256]{0,1:T(8,128)(2,1)S(1)}, u32[]{:S(2)}, u32[]{:S(2)}) collective-permute-start(bf16[384,256]{0,1:T(8,128)(2,1)S(1)} %collective-permute-done), channel_id=1, source_target_pairs={{0,4},{4,8},{8,12},{12,16},{16,20},{20,24},{24,28},{28,0},{1,5},{5... | collective-permute-start | bytes 589832 | tf_op jit(solution)/shard_map/ppermute | solution.py:96
  33.2 8.4 %collective-permute-start.2 = (bf16[384,256]{0,1:T(8,128)(2,1)S(1)}, bf16[384,256]{0,1:T(8,128)(2,1)S(1)}, u32[]{:S(2)}, u32[]{:S(2)}) collective-permute-start(bf16[384,256]{0,1:T(8,128)(2,1)S(1)} %collective-permute-done.1), channel_id=1, source_target_pairs={{0,4},{4,8},{8,12},{12,16},{16,20},{20,24},{24,28},{28,0},{1,5},{5... | collective-permute-start | bytes 589832 | tf_op jit(solution)/shard_map/ppermute | solution.py:96
  41.5 13.5 %collective-permute-start.3 = (bf16[384,256]{0,1:T(8,128)(2,1)S(1)}, bf16[384,256]{0,1:T(8,128)(2,1)S(1)}, u32[]{:S(2)}, u32[]{:S(2)}) collective-permute-start(bf16[384,256]{0,1:T(8,128)(2,1)S(1)} %collective-permute-done.2), channel_id=1, source_target_pairs={{0,4},{4,8},{8,12},{12,16},{16,20},{20,24},{24,28},{28,0},{1,5},{5... | collective-permute-start | bytes 589832 | tf_op jit(solution)/shard_map/ppermute | solution.py:96
  55.1 11.5 %collective-permute-start.4 = (bf16[384,256]{0,1:T(8,128)(2,1)S(1)}, bf16[384,256]{0,1:T(8,128)(2,1)S(1)}, u32[]{:S(2)}, u32[]{:S(2)}) collective-permute-start(bf16[384,256]{0,1:T(8,128)(2,1)S(1)} %collective-permute-done.3), channel_id=1, source_target_pairs={{0,4},{4,8},{8,12},{12,16},{16,20},{20,24},{24,28},{28,0},{1,5},{5... | collective-permute-start | bytes 589832 | tf_op jit(solution)/shard_map/ppermute | solution.py:96
  66.6 10.2 %collective-permute-start.5 = (bf16[384,256]{0,1:T(8,128)(2,1)S(1)}, bf16[384,256]{0,1:T(8,128)(2,1)}, u32[]{:S(2)}, u32[]{:S(2)}) collective-permute-start(bf16[384,256]{0,1:T(8,128)(2,1)S(1)} %collective-permute-done.4), channel_id=1, source_target_pairs={{0,4},{4,8},{8,12},{12,16},{16,20},{20,24},{24,28},{28,0},{1,5},{5... | collective-permute-start | bytes 589832 | tf_op jit(solution)/shard_map/ppermute | solution.py:96
  76.8 8.6 %collective-permute-start.6 = (bf16[384,256]{0,1:T(8,128)(2,1)}, bf16[384,256]{0,1:T(8,128)(2,1)S(1)}, u32[]{:S(2)}, u32[]{:S(2)}) collective-permute-start(bf16[384,256]{0,1:T(8,128)(2,1)} %collective-permute-done.5), channel_id=1, source_target_pairs={{0,4},{4,8},{8,12},{12,16},{16,20},{20,24},{24,28},{28,0},{1,5},{5... | collective-permute-start | bytes 589832 | tf_op jit(solution)/shard_map/ppermute | solution.py:96
  104.8 0.9 copy-start.1
  106.5 3.7 %copy-start.2 = (f32[2,384,2,128]{3,1,0,2:T(8,128)S(1)}, f32[2,384,2,128]{3,1,0,2:T(8,128)}, u32[]{:S(2)}) copy-start(f32[2,384,2,128]{3,1,0,2:T(8,128)} %copy-done.1) | copy-start | bytes 2359300
  110.3 11.9 %copy-start.5 = (bf16[96,2048]{1,0:T(8,128)(2,1)S(1)}, bf16[96,2048]{1,0:T(8,128)(2,1)}, u32[]{:S(2)}) copy-start(bf16[96,2048]{1,0:T(8,128)(2,1)} %param.23) | copy-start | bytes 1179652
  113.3 12.9 %copy-start.7 = (f32[2048]{0:T(1024)S(1)}, f32[2048]{0:T(1024)}, u32[]{:S(2)}) copy-start(f32[2048]{0:T(1024)} %param.24) | copy-start | bytes 24580
  113.4 8.8 %all-to-all-start = ((bf16[4,96,256]{2,1,0:T(8,128)(2,1)}), bf16[4,96,256]{2,1,0:T(8,128)(2,1)S(1)}, u32[]{:S(2)}, u32[]{:S(2)}) async-start(bf16[4,96,256]{2,1,0:T(8,128)(2,1)} %multiply_convert_fusion.2), calls=%async_computation | async-start | bytes 393216 | tf_op jit(solution)/shard_map/all_to_all | solution.py:122
  116.9 100.7 %all-gather.8.cloned.1.call-start = ((), (), s32[]{:S(2)}) async-start(), calls=%async_computation.6 | async-start | bytes 4915200 | tf_op jit(solution)/shard_map/all_gather | solution.py:146
  125.3 0.9 copy-start.3
  185.9 90.9 %reduce-scatter.2.cloned.1.call-start = ((), (), s32[]{:S(2)}) async-start(), calls=%async_computation.7 | async-start | bytes 4915200 | tf_op jit(solution)/shard_map/reduce_scatter | solution.py:152
  233.7 51.1 %copy-start.6 = (f32[96,2]{0,1:T(2,128)S(1)}, f32[96,2]{0,1:T(2,128)}, u32[]{:S(2)}) copy-start(f32[96,2]{0,1:T(2,128)} %param.26) | copy-start | bytes 2308
  279.3 31.3 %all-to-all-start.2 = ((bf16[8,30,2048]{2,1,0:T(8,128)(2,1)}), bf16[8,30,2048]{2,1,0:T(8,128)(2,1)}, u32[]{:S(2)}, u32[]{:S(2)}) async-start(bf16[8,30,2048]{2,1,0:T(8,128)(2,1)} %reshape.160), calls=%async_computation.3 | async-start | bytes 2097152 | tf_op jit(solution)/shard_map/all_to_all | solution.py:159
  314.1 6.8 %copy-start.4 = (f32[96,2048]{1,0:T(8,128)S(1)}, f32[96,2048]{1,0:T(8,128)}, u32[]{:S(2)}) copy-start(f32[96,2048]{1,0:T(8,128)} %copy-done.3) | copy-start | bytes 2359300
Sparse Core Ops, SparseCore 0:
  9.4 54.1 all-gather.3
  65.1 35.0 all-gather.5
  186.0 31.4 all-gather.7
  233.9 42.9 reduce-scatter.1
